TPU v7x, 512 devices: a 4x2x32 block of a 4x8x32 slice. The times are simulated.
512 devices in a mesh: grp: 2 (over y), fs: 32 (over z), tp: 8 (over x, core).
Axes of the slice: x: 4, y: 2, z: 32, core: 2. Of those that a mesh axis runs over, the one named last changes fastest.
The devices are a block of a 4x8x32 slice.
Arguments:
- tokens: bfloat16 [24576, 2048], P(('grp', 'fs'), 'tp'), parts along dimension 0, may hold values from -6 to 6
- mix_gain: float32 [2048], replicated, may hold values from 0.1 to 1.9
- w_signal: bfloat16 [2048, 1024], P('fs', 'tp'), may hold values from -0.125 to 0.125
- w_outer_gate: bfloat16 [2048, 1024], P('fs', 'tp'), may hold values from -0.125 to 0.125
- w_inner_gate: bfloat16 [2048, 1024], P('fs', 'tp'), may hold values from -0.125 to 0.125
- mix_taps: float32 [3, 1024], P(None, 'tp'), may hold values from -3 to 3
- w_mix_out: bfloat16 [1024, 2048], P('tp', 'fs'), may hold values from -0.1875 to 0.1875
- ffn_gain: float32 [2048], replicated, may hold values from 0.1 to 1.9
- w_gate: bfloat16 [2048, 5120], P('fs', 'tp'), may hold values from -0.125 to 0.125
- w_value: bfloat16 [2048, 5120], P('fs', 'tp'), may hold values from -0.125 to 0.125
- up_taps: float32 [2, 3, 5120], P(None, None, 'tp'), may hold values from -3 to 3
- up_bias: float32 [2, 5120], P(None, 'tp'), may hold values from -3 to 3
- w_down: bfloat16 [5120, 2048], P('tp', 'fs'), may hold values from -0.078125 to 0.078125
Outputs:
- layer_out: bfloat16 [24576, 2048], P(('grp', 'fs'), 'tp'), parts along dimension 0
There are 2 independent parts, one for each index of `grp`. A program takes and returns all parts, laid end to end along the dimension named above; an argument that names none is the same for every part. Nothing has to cross between parts.
All inputs are finite; a program needn't handle non-finite values.
Results may differ from a plain program's by a relative error of at most 0.022.
Values may be sent and summed in bfloat16 or wider, within the bound.
A program may use at most 64 MiB of HBM per device.

v0:
```python
import jax
import jax.numpy as jnp
from jax import lax
from jax.sharding import PartitionSpec as P

SEQS_DEV = 2


def in_one_piece(arrays, axis, dim, along):
    widths = [a.shape[along] for a in arrays]
    both = jnp.concatenate(arrays, axis=along)
    filled = lax.all_gather(both, axis, axis=dim, tiled=True)
    return tuple(jnp.split(filled, [sum(widths[:k]) for k in range(1, len(widths))], axis=along))


def copy_for_each(value, axis):
    copies = jnp.broadcast_to(value, (lax.axis_size(axis), *value.shape))
    return lax.all_to_all(copies, axis, split_axis=0, concat_axis=0, tiled=True)


def in_order(pieces, dim):
    shape = list(pieces.shape[1:])
    shape[dim] *= pieces.shape[0]
    return jnp.moveaxis(pieces, 0, dim).reshape(shape)


def gathered_copies(value, axis, dim):
    pieces = copy_for_each(value, axis)
    return in_order(pieces, dim)


def split_up(value, dim, devices):
    shape = value.shape
    pieces = value.reshape(*shape[:dim], devices, shape[dim] // devices, *shape[dim + 1 :])
    return jnp.moveaxis(pieces, dim, 0)


def sent_and_summed(value, axis, dim):
    devices = lax.axis_size(axis)
    pieces = lax.all_to_all(split_up(value, dim, devices), axis, 0, 0, tiled=True)
    return jnp.sum(pieces.astype(jnp.float32), axis=0)


def conv_positions(values, taps):
    width = values.shape[1]
    blocks = values.reshape(SEQS_DEV, -1, width)
    length = blocks.shape[1]
    padded = jnp.pad(blocks, ((0, 0), (2, 0), (0, 0)))
    result = (
        padded[:, 0:length] * taps[0]
        + padded[:, 1 : length + 1] * taps[1]
        + padded[:, 2 : length + 2] * taps[2]
    )
    return result.reshape(-1, width)


def rms_norm(stream, gain):
    values = stream.astype(jnp.float32)
    scale = lax.rsqrt(jnp.mean(values * values, axis=-1, keepdims=True) + 1e-06)
    return (values * scale * gain).astype(jnp.bfloat16)


def on_device(
    tokens,
    mix_gain,
    w_signal,
    w_outer_gate,
    w_inner_gate,
    mix_taps,
    w_mix_out,
    ffn_gain,
    w_gate,
    w_value,
    up_taps,
    up_bias,
    w_down,
):
    gate_full, value_full = in_one_piece((w_gate, w_value), "fs", 0, 1)
    whole = gathered_copies(tokens, "tp", 1)
    normed = rms_norm(whole, mix_gain)
    signal_full, outer_full, inner_full = in_one_piece(
        (w_signal, w_outer_gate, w_inner_gate), "fs", 0, 1
    )
    signal = jnp.dot(normed, signal_full, preferred_element_type=jnp.float32)
    outer = jnp.dot(normed, outer_full, preferred_element_type=jnp.float32)
    inner = jnp.dot(normed, inner_full, preferred_element_type=jnp.float32)
    signal = signal.astype(jnp.bfloat16).astype(jnp.float32)
    outer = outer.astype(jnp.bfloat16).astype(jnp.float32)
    inner = inner.astype(jnp.bfloat16).astype(jnp.float32)
    mixed = (outer * conv_positions(inner * signal, mix_taps)).astype(jnp.bfloat16)
    mix_terms = jnp.dot(
        mixed,
        lax.all_gather(w_mix_out, "fs", axis=1, tiled=True),
        preferred_element_type=jnp.float32,
    )
    mix_sum = sent_and_summed(mix_terms.astype(jnp.bfloat16), "tp", 1)
    resid = (tokens.astype(jnp.float32) + mix_sum).astype(jnp.bfloat16)
    whole_ffn = gathered_copies(resid, "tp", 1)
    normed_ffn = rms_norm(whole_ffn, ffn_gain)
    gate = jnp.dot(normed_ffn, gate_full, preferred_element_type=jnp.float32)
    value = jnp.dot(normed_ffn, value_full, preferred_element_type=jnp.float32)
    gate = gate.astype(jnp.bfloat16).astype(jnp.float32)
    value = value.astype(jnp.bfloat16).astype(jnp.float32)
    gate_conv = conv_positions(gate, up_taps[0]) + up_bias[0]
    value_conv = conv_positions(value, up_taps[1]) + up_bias[1]
    hidden = (jax.nn.silu(gate_conv) * value_conv).astype(jnp.bfloat16)
    ffn_terms = jnp.dot(
        hidden, lax.all_gather(w_down, "fs", axis=1, tiled=True), preferred_element_type=jnp.float32
    )
    ffn_sum = sent_and_summed(ffn_terms.astype(jnp.bfloat16), "tp", 1)
    return (resid.astype(jnp.float32) + ffn_sum).astype(jnp.bfloat16)


def solution(mesh):
    placed = (
        P(("grp", "fs"), "tp"),
        P(),
        P("fs", "tp"),
        P("fs", "tp"),
        P("fs", "tp"),
        P(None, "tp"),
        P("tp", "fs"),
        P(),
        P("fs", "tp"),
        P("fs", "tp"),
        P(None, None, "tp"),
        P(None, "tp"),
        P("tp", "fs"),
    )
    return jax.shard_map(
        on_device, mesh=mesh, in_specs=placed, out_specs=P(("grp", "fs"), "tp"), check_vma=False
    )
```

profile of v0, /device:TPU:33, one launch (start us, length us, event | category | flops | bytes accessed | tf_op | source)
XLA Modules:
  0.0 474.6 jit_solution(4301556435789790506)
XLA Ops:
  6.6 1.4 pad_maximum_fusion.1
  8.1 1.6 pad_maximum_fusion
  9.7 1.1 copy.16
  10.8 1.3 broadcast_in_dim.4
  12.1 45.1 %all-to-all-start = ((bf16[8,384,256]{1,2,0:T(8,128)(2,1)}), bf16[8,384,256]{1,2,0:T(8,128)(2,1)S(1)}, u32[]{:S(2)}, u32[]{:S(2)}) async-start(bf16[8,384,256]{1,2,0:T(8,128)(2,1)} %broadcast_in_dim.4), calls=%async_computation | async-start | bytes 3145728 | tf_op jit(solution)/shard_map/all_to_all | solution.py:18
  57.2 52.2 %all_gather.13 = bf16[128,2048]{0,1:T(8,128)(2,1)} all-gather(bf16[128,64]{0,1:T(8,128)(2,1)S(1)} %copy-done.1), channel_id=1, replica_groups=mesh['grp'=2,'fs'=32,'tp'=8] {'fs'}, dimensions={1}, use_global_device_ids=true | all-gather | bytes 540672 | tf_op jit(solution)/shard_map/all_gather | solution.py:93
  110.3 39.8 %all-gather.4.cloned.1.call-done = bf16[2048,384]{1,0:T(8,128)(2,1)} async-done(((bf16[64,384]{1,0:T(8,128)(2,1)}), bf16[2048,384]{1,0:T(8,128)(2,1)}) %all-gather.4.cloned.1.call-update) | async-done | bytes 1572880 | tf_op jit(solution)/shard_map/all_gather | solution.py:12
  150.0 1.7 fusion.16
  151.7 1.7 fusion.15
  153.5 3.0 convolution_convert_fusion.1
  156.5 1.3 copy.25
  157.8 25.3 %all-to-all-start.1 = ((bf16[8,384,256]{2,1,0:T(8,128)(2,1)}), bf16[8,384,256]{2,1,0:T(8,128)(2,1)S(1)}, u32[]{:S(2)}, u32[]{:S(2)}) async-start(bf16[8,384,256]{2,1,0:T(8,128)(2,1)} %bitcast.59), calls=%async_computation.1 | async-start | bytes 3145728 | tf_op jit(solution)/shard_map/all_to_all | solution.py:40
  183.1 0.7 all-gather.8.cloned.1.call-update
  183.9 19.8 %all-to-all-done.1 = bf16[8,384,256]{2,1,0:T(8,128)(2,1)S(1)} async-done(((bf16[8,384,256]{2,1,0:T(8,128)(2,1)}), bf16[8,384,256]{2,1,0:T(8,128)(2,1)S(1)}, u32[]{:S(2)}, u32[]{:S(2)}) %all-to-all-start.1) | async-done | bytes 1572896 | tf_op jit(solution)/shard_map/all_to_all | solution.py:40
  204.2 1.4 broadcast_in_dim.5
  205.5 4.6 all-to-all-start.2
  210.2 20.6 %all-to-all-done.2 = bf16[8,384,256]{1,2,0:T(8,128)(2,1)S(1)} async-done(((bf16[8,384,256]{1,2,0:T(8,128)(2,1)}), bf16[8,384,256]{1,2,0:T(8,128)(2,1)S(1)}, u32[]{:S(2)}, u32[]{:S(2)}) %all-to-all-start.2) | async-done | bytes 1572896 | tf_op jit(solution)/shard_map/all_to_all | solution.py:18
  231.7 56.5 %all-gather.6.cloned.1.call-done = bf16[2048,1280]{1,0:T(8,128)(2,1)} async-done(((bf16[64,1280]{1,0:T(8,128)(2,1)}), bf16[2048,1280]{1,0:T(8,128)(2,1)}) %all-gather.6.cloned.1.call-update) | async-done | bytes 5242896 | tf_op jit(solution)/shard_map/all_gather | solution.py:12
  288.2 3.3 fusion.8
  291.6 1.4 fusion.11
  294.0 124.1 %all-gather.8.cloned.1.call-done = bf16[640,2048]{0,1:T(8,128)(2,1)} async-done(((bf16[640,64]{0,1:T(8,128)(2,1)}), bf16[640,2048]{0,1:T(8,128)(2,1)}) %all-gather.8.cloned.1.call-update) | async-done | bytes 2621456 | tf_op jit(solution)/shard_map/all_gather | solution.py:108
  418.1 3.2 convolution_convert_fusion
  421.4 45.7 %all_to_all.20 = bf16[8,384,256]{2,1,0:T(8,128)(2,1)S(1)} all-to-all(bf16[8,384,256]{2,1,0:T(8,128)(2,1)S(1)} %bitcast.61), channel_id=1, replica_groups=mesh['grp'=2,'fs'=32,'tp'=8] {'tp'}, dimensions={0} | all-to-all | bytes 3145728 | tf_op jit(solution)/shard_map/all_to_all | solution.py:40
  467.3 0.7 add_convert_fusion
  (41 shorter events, 3.8 us)
Async XLA Ops:
  6.5 143.5 %all-gather.4.cloned.1.call-start = ((), (), s32[]{:S(2)}) async-start(), calls=%async_computation.4 | async-start | bytes 1622016 | tf_op jit(solution)/shard_map/all_gather | solution.py:12
  8.0 280.2 %all-gather.6.cloned.1.call-start = ((), (), s32[]{:S(2)}) async-start(), calls=%async_computation.5 | async-start | bytes 5406720 | tf_op jit(solution)/shard_map/all_gather | solution.py:12
  12.1 45.1 %copy-start.6 = (f32[3,128]{1,0:T(4,128)S(1)}, f32[3,128]{1,0:T(4,128)}, u32[]{:S(2)}) copy-start(f32[3,128]{1,0:T(4,128)} %param.18) | copy-start | bytes 4612
  12.1 45.1 %copy-start.1 = (bf16[128,64]{0,1:T(8,128)(2,1)S(1)}, bf16[128,64]{0,1:T(8,128)(2,1)}, u32[]{:S(2)}) copy-start(bf16[128,64]{0,1:T(8,128)(2,1)} %param.19) | copy-start | bytes 49156
  12.1 97.3 %all-to-all-start = ((bf16[8,384,256]{1,2,0:T(8,128)(2,1)}), bf16[8,384,256]{1,2,0:T(8,128)(2,1)S(1)}, u32[]{:S(2)}, u32[]{:S(2)}) async-start(bf16[8,384,256]{1,2,0:T(8,128)(2,1)} %broadcast_in_dim.4), calls=%async_computation | async-start | bytes 3145728 | tf_op jit(solution)/shard_map/all_to_all | solution.py:18
  57.2 52.7 %copy-start.3 = (f32[2048]{0:T(1024)S(1)}, f32[2048]{0:T(1024)}, u32[]{:S(2)}) copy-start(f32[2048]{0:T(1024)} %param.14) | copy-start | bytes 24580
  157.8 45.9 %all-to-all-start.1 = ((bf16[8,384,256]{2,1,0:T(8,128)(2,1)}), bf16[8,384,256]{2,1,0:T(8,128)(2,1)S(1)}, u32[]{:S(2)}, u32[]{:S(2)}) async-start(bf16[8,384,256]{2,1,0:T(8,128)(2,1)} %bitcast.59), calls=%async_computation.1 | async-start | bytes 3145728 | tf_op jit(solution)/shard_map/all_to_all | solution.py:40
  183.1 20.8 %copy-start = (bf16[384,256]{1,0:T(8,128)(2,1)S(1)}, bf16[384,256]{1,0:T(8,128)(2,1)}, u32[]{:S(2)}) copy-start(bf16[384,256]{1,0:T(8,128)(2,1)} %param.13) | copy-start | bytes 589828
  183.1 235.0 %all-gather.8.cloned.1.call-start = ((), (), s32[]{:S(2)}) async-start(), calls=%async_computation.6 | async-start | bytes 2703360 | tf_op jit(solution)/shard_map/all_gather | solution.py:108
  205.5 4.6 copy-start.5
  205.5 4.6 copy-start.2
  205.5 25.3 %all-to-all-start.2 = ((bf16[8,384,256]{1,2,0:T(8,128)(2,1)}), bf16[8,384,256]{1,2,0:T(8,128)(2,1)S(1)}, u32[]{:S(2)}, u32[]{:S(2)}) async-start(bf16[8,384,256]{1,2,0:T(8,128)(2,1)} %broadcast_in_dim.5), calls=%async_computation.2 | async-start | bytes 3145728 | tf_op jit(solution)/shard_map/all_to_all | solution.py:18
  210.1 21.1 %copy-start.4 = (f32[2048]{0:T(1024)S(1)}, f32[2048]{0:T(1024)}, u32[]{:S(2)}) copy-start(f32[2048]{0:T(1024)} %param.20) | copy-start | bytes 24580
  288.2 3.4 copy-start.7
Sparse Core Ops, SparseCore 0:
  9.4 140.5 all-gather.3
  152.1 135.9 all-gather.5
  290.3 127.7 all-gather.7
where the time goes:
time: 475 us
  waiting for transfers between devices  262 us (55%)
  blocking collectives  98 us (21%)
  starting transfers between devices  75.1 us (16%)
  matrix products  14.3 us (3%)
  between operations  13.3 us (3%)
  other arithmetic  6.94 us (1%)
  local copies, waits for them, and re-layouts  5.44 us (1%)
    all_gather x1, waiting for transfers between devices, on_device(): lax.all_gather(w_down, 'fs', axis=1, tiled=True)  124 us
    all_gather x2, waiting for transfers between devices, in_one_piece(): filled = lax.all_gather(both, axis, axis=dim, tiled=True)  96.2 us
    all_gather x1, blocking collectives, on_device(): lax.all_gather(w_mix_out, 'fs', axis=1, tiled=True)  52.2 us
    all_to_all x2, starting transfers between devices, copy_for_each(): return lax.all_to_all(copies, axis, split_axis=0, concat_axis=0, tiled=True)  49.7 us
    all_to_all x1, blocking collectives, sent_and_summed(): lax.all_to_all(split_up(value, dim, devices), axis, 0, 0, tiled=True)  45.7 us
    all_to_all x1, starting transfers between devices, sent_and_summed(): lax.all_to_all(split_up(value, dim, devices), axis, 0, 0, tiled=True)  25.3 us
    all_to_all x2, waiting for transfers between devices, copy_for_each(): return lax.all_to_all(copies, axis, split_axis=0, concat_axis=0, tiled=True)  20.6 us
    all_to_all x1, waiting for transfers between devices, sent_and_summed(): lax.all_to_all(split_up(value, dim, devices), axis, 0, 0, tiled=True)  19.8 us
  transfers between devices with their start and end apart: 6, of which 5 were waited for; matrix products, arithmetic and copies ran while one was open for 4% of the time, Pallas kernels for 0%

commit v1 on v0

--- a/solution.py
+++ b/solution.py
@@ -105,7 +105,11 @@
     value_conv = conv_positions(value, up_taps[1]) + up_bias[1]
     hidden = (jax.nn.silu(gate_conv) * value_conv).astype(jnp.bfloat16)
     ffn_terms = jnp.dot(
-        hidden, lax.all_gather(w_down, "fs", axis=1, tiled=True), preferred_element_type=jnp.float32
+        hidden,
+        jnp.concatenate(
+            lax.all_to_all(jnp.stack([w_down] * lax.axis_size("fs")), "fs", 0, 0), axis=1
+        ),
+        preferred_element_type=jnp.float32,
     )
     ffn_sum = sent_and_summed(ffn_terms.astype(jnp.bfloat16), "tp", 1)
     return (resid.astype(jnp.float32) + ffn_sum).astype(jnp.bfloat16)

time: 475 us -> 603 us (1.27)
  waiting for transfers between devices: 262 us -> 347 us
  blocking collectives: 98 us -> 158 us
  starting transfers between devices: 75.1 us -> 58.3 us
    all_gather x2, waiting for transfers between devices: 96.2 us -> 347 us  [in_one_piece(): filled = lax.all_gather(both, axis, axis=dim, tiled=True)]
    all_gather x1 -> x0, waiting for transfers between devices: 124 us -> none  [on_device(): lax.all_gather(w_down, 'fs', axis=1, tiled=True)]
    all_to_all x1 -> x2, blocking collectives: 45.7 us -> 81.6 us  [sent_and_summed(): lax.all_to_all(split_up(value, dim, devices), axis, 0, 0, tiled=True)]
    all_to_all x0 -> x1, blocking collectives: none -> 24.2 us  [copy_for_each(): return lax.all_to_all(copies, axis, split_axis=0, concat_axis=0, tiled=True)]
    all_to_all x2 -> x1, waiting for transfers between devices: 20.6 us -> 0.01 us  [copy_for_each(): return lax.all_to_all(copies, axis, split_axis=0, concat_axis=0, tiled=True)]
    all_to_all x1, waiting for transfers between devices: 19.8 us -> 0.01 us  [on_device(): lax.all_to_all(jnp.stack([w_down] * lax.axis_size('fs')), 'fs', 0, 0)]
    all_to_all x1, starting transfers between devices: 25.3 us -> 13 us  [on_device(): lax.all_to_all(jnp.stack([w_down] * lax.axis_size('fs')), 'fs', 0, 0)]
    all_to_all x2 -> x1, starting transfers between devices: 49.7 us -> 45.1 us  [copy_for_each(): return lax.all_to_all(copies, axis, split_axis=0, concat_axis=0, tiled=True)]
  transfers between devices with their start and end apart: 6 -> 4, of which waited for: 5 -> 2; matrix products, arithmetic and copies ran while one was open for 4% -> 2% of each run, Pallas kernels for 0% -> 0%
where the time goes in v1:
time: 603 us; the launch traced here: 602 us
  waiting for transfers between devices  347 us (58%)
  blocking collectives  158 us (26%)
  starting transfers between devices  58.3 us (10%)
  matrix products  14.3 us (2%)
  between operations  13.7 us (2%)
    all_gather x2, waiting for transfers between devices, in_one_piece(): filled = lax.all_gather(both, axis, axis=dim, tiled=True)  347 us
    all_to_all x2, blocking collectives, sent_and_summed(): lax.all_to_all(split_up(value, dim, devices), axis, 0, 0, tiled=True)  81.6 us
    all_gather x1, blocking collectives, on_device(): lax.all_gather(w_mix_out, 'fs', axis=1, tiled=True)  51.7 us
    all_to_all x1, starting transfers between devices, copy_for_each(): return lax.all_to_all(copies, axis, split_axis=0, concat_axis=0, tiled=True)  45.1 us
    all_to_all x1, blocking collectives, copy_for_each(): return lax.all_to_all(copies, axis, split_axis=0, concat_axis=0, tiled=True)  24.2 us
    all_to_all x1, starting transfers between devices, on_device(): lax.all_to_all(jnp.stack([w_down] * lax.axis_size('fs')), 'fs', 0, 0)  13 us
  transfers between devices with their start and end apart: 4, of which 2 were waited for; matrix products, arithmetic and copies ran while one was open for 2% of the time, Pallas kernels for 0%

profile of v1, /device:TPU:33, one launch (start us, length us, event | category | flops | bytes accessed | tf_op | source)
XLA Modules:
  0.0 602.4 jit_solution(1533080965248781350)
XLA Ops:
  6.6 1.4 pad_maximum_fusion.1
  8.0 1.1 copy.17
  9.1 1.3 broadcast_in_dim.4
  10.4 45.1 %all-to-all-start = ((bf16[8,384,256]{1,2,0:T(8,128)(2,1)}), bf16[8,384,256]{1,2,0:T(8,128)(2,1)S(1)}, u32[]{:S(2)}, u32[]{:S(2)}) async-start(bf16[8,384,256]{1,2,0:T(8,128)(2,1)} %broadcast_in_dim.4), calls=%async_computation | async-start | bytes 3145728 | tf_op jit(solution)/shard_map/all_to_all | solution.py:18
  55.5 51.7 %all_gather.10 = bf16[128,2048]{0,1:T(8,128)(2,1)} all-gather(bf16[128,64]{0,1:T(8,128)(2,1)S(1)} %copy-done.4), channel_id=1, replica_groups=mesh['grp'=2,'fs'=32,'tp'=8] {'fs'}, dimensions={1}, use_global_device_ids=true | all-gather | bytes 540672 | tf_op jit(solution)/shard_map/all_gather | solution.py:93
  107.2 0.4 multiply_reduce_fusion.1
  107.6 0.4 fusion.3
  108.0 41.5 %all-gather.3.cloned.1.call-done = bf16[2048,384]{1,0:T(8,128)(2,1)} async-done(((bf16[64,384]{1,0:T(8,128)(2,1)}), bf16[2048,384]{1,0:T(8,128)(2,1)}) %all-gather.3.cloned.1.call-update) | async-done | bytes 1572880 | tf_op jit(solution)/shard_map/all_gather | solution.py:12
  149.5 1.7 fusion.16
  151.2 1.7 fusion.15
  152.9 3.0 convolution_convert_fusion.1
  156.1 46.7 %all_to_all.25 = bf16[8,384,256]{2,1,0:T(8,128)(2,1)S(1)} all-to-all(bf16[8,384,256]{2,1,0:T(8,128)(2,1)S(1)} %bitcast.55), channel_id=1, replica_groups=mesh['grp'=2,'fs'=32,'tp'=8] {'tp'}, dimensions={0} | all-to-all | bytes 3145728 | tf_op jit(solution)/shard_map/all_to_all | solution.py:40
  202.9 0.7 copy-done
  204.0 24.2 %all_to_all.26 = bf16[8,384,256]{1,2,0:T(8,128)(2,1)S(1)} all-to-all(bf16[8,384,256]{1,2,0:T(8,128)(2,1)S(1)} %broadcast_in_dim.5), channel_id=1, replica_groups=mesh['grp'=2,'fs'=32,'tp'=8] {'tp'}, dimensions={0} | all-to-all | bytes 3145728 | tf_op jit(solution)/shard_map/all_to_all | solution.py:18
  228.3 1.9 stack.2
  230.2 13.0 %all-to-all-start.3 = ((bf16[32,640,64]{1,2,0:T(8,128)(2,1)}), bf16[32,640,64]{1,2,0:T(8,128)(2,1)}, u32[]{:S(2)}, u32[]{:S(2)}) async-start(bf16[32,640,64]{1,2,0:T(8,128)(2,1)} %stack.2), calls=%async_computation.3 | async-start | bytes 5242880 | tf_op jit(solution)/shard_map/all_to_all | solution.py:110
  243.5 0.7 pad_maximum_fusion
  245.2 305.4 %all-gather.5.cloned.1.call-done = bf16[2048,1280]{1,0:T(8,128)(2,1)} async-done(((bf16[64,1280]{1,0:T(8,128)(2,1)}), bf16[2048,1280]{1,0:T(8,128)(2,1)}) %all-gather.5.cloned.1.call-update) | async-done | bytes 5242896 | tf_op jit(solution)/shard_map/all_gather | solution.py:12
  550.6 3.3 fusion.8
  554.0 1.4 fusion.11
  555.6 0.9 fusion.30
  556.4 3.2 convolution_convert_fusion
  559.7 34.9 %all_to_all.27 = bf16[8,384,256]{2,1,0:T(8,128)(2,1)S(1)} all-to-all(bf16[8,384,256]{2,1,0:T(8,128)(2,1)S(1)} %bitcast.56), channel_id=1, replica_groups=mesh['grp'=2,'fs'=32,'tp'=8] {'tp'}, dimensions={0} | all-to-all | bytes 3145728 | tf_op jit(solution)/shard_map/all_to_all | solution.py:40
  594.9 0.7 add_convert_fusion
  (44 shorter events, 2.5 us)
Async XLA Ops:
  6.5 143.0 %all-gather.3.cloned.1.call-start = ((), (), s32[]{:S(2)}) async-start(), calls=%async_computation.5 | async-start | bytes 1622016 | tf_op jit(solution)/shard_map/all_gather | solution.py:12
  10.4 45.1 %copy-start.9 = (f32[3,128]{1,0:T(4,128)S(1)}, f32[3,128]{1,0:T(4,128)}, u32[]{:S(2)}) copy-start(f32[3,128]{1,0:T(4,128)} %param.18) | copy-start | bytes 4612
  10.4 45.1 %copy-start.4 = (bf16[128,64]{0,1:T(8,128)(2,1)S(1)}, bf16[128,64]{0,1:T(8,128)(2,1)}, u32[]{:S(2)}) copy-start(bf16[128,64]{0,1:T(8,128)(2,1)} %param.19) | copy-start | bytes 49156
  10.4 96.8 %all-to-all-start = ((bf16[8,384,256]{1,2,0:T(8,128)(2,1)}), bf16[8,384,256]{1,2,0:T(8,128)(2,1)S(1)}, u32[]{:S(2)}, u32[]{:S(2)}) async-start(bf16[8,384,256]{1,2,0:T(8,128)(2,1)} %broadcast_in_dim.4), calls=%async_computation | async-start | bytes 3145728 | tf_op jit(solution)/shard_map/all_to_all | solution.py:18
  55.4 52.2 %copy-start.6 = (f32[2048]{0:T(1024)S(1)}, f32[2048]{0:T(1024)}, u32[]{:S(2)}) copy-start(f32[2048]{0:T(1024)} %param.14) | copy-start | bytes 24580
  202.7 0.9 copy-start
  204.0 24.3 %copy-start.3 = (bf16[640,64]{0,1:T(8,128)(2,1)S(1)}, bf16[640,64]{0,1:T(8,128)(2,1)}, u32[]{:S(2)}) copy-start(bf16[640,64]{0,1:T(8,128)(2,1)} %param.25) | copy-start | bytes 245764
  230.2 13.3 %copy-start.1 = (bf16[64,640]{1,0:T(8,128)(2,1)S(1)}, bf16[64,640]{1,0:T(8,128)(2,1)}, u32[]{:S(2)}) copy-start(bf16[64,640]{1,0:T(8,128)(2,1)} %param.22) | copy-start | bytes 245764
  230.2 13.3 %copy-start.2 = (bf16[64,640]{1,0:T(8,128)(2,1)S(1)}, bf16[64,640]{1,0:T(8,128)(2,1)}, u32[]{:S(2)}) copy-start(bf16[64,640]{1,0:T(8,128)(2,1)} %param.21) | copy-start | bytes 245764
  230.2 14.0 %copy-start.8 = (f32[2,640]{1,0:T(2,128)S(1)}, f32[2,640]{1,0:T(2,128)}, u32[]{:S(2)}) copy-start(f32[2,640]{1,0:T(2,128)} %param.24) | copy-start | bytes 15364
  230.2 14.1 %copy-start.5 = (f32[2,3,640]{2,0,1:T(2,128)S(1)}, f32[2,3,640]{2,0,1:T(2,128)}, u32[]{:S(2)}) copy-start(f32[2,3,640]{2,0,1:T(2,128)} %param.23) | copy-start | bytes 46084
  230.2 326.2 %all-to-all-start.3 = ((bf16[32,640,64]{1,2,0:T(8,128)(2,1)}), bf16[32,640,64]{1,2,0:T(8,128)(2,1)}, u32[]{:S(2)}, u32[]{:S(2)}) async-start(bf16[32,640,64]{1,2,0:T(8,128)(2,1)} %stack.2), calls=%async_computation.3 | async-start | bytes 5242880 | tf_op jit(solution)/shard_map/all_to_all | solution.py:110
  243.2 1.6 copy-start.7
  243.2 307.4 %all-gather.5.cloned.1.call-start = ((), (), s32[]{:S(2)}) async-start(), calls=%async_computation.6 | async-start | bytes 5406720 | tf_op jit(solution)/shard_map/all_gather | solution.py:12
  550.6 3.4 copy-start.10
Sparse Core Ops, SparseCore 0:
  9.4 140.0 all-gather.2
  246.1 304.4 all-gather.4
